TPU v7x, 32 devices: a whole 2x2x4 slice. The times are simulated.
32 devices in a mesh: sp: 16 (over z, y, x), tp: 2 (over core).
Axes of the slice: x: 2, y: 2, z: 4, core: 2. Of those that a mesh axis runs over, the one named last changes fastest.
Arguments:
- queries: bfloat16 [4096, 1024], P('sp', 'tp'), may hold values from -100 to 100
- keys: bfloat16 [256, 4096], P('tp', 'sp'), may hold values from -5 to 5
- values: bfloat16 [256, 4096], P('tp', 'sp'), may hold values from -4.5 to 4.5
- gate_cache: float32 [8, 4096], P('tp', 'sp'), as said below
- documents: int32 [4096], P('sp'), may hold values from 0 to 2, never falling along the last dimension, each value on 1 to 2560 neighbouring positions
- residual: bfloat16 [4096, 2048], P(('sp', 'tp')), may hold values from -3 to 3
- out_weight: bfloat16 [1024, 2048], replicated, may hold values from -2 to 2
- mix_gain: bfloat16 [2048], replicated, may hold values from 0.099609375 to 1.8984375
- routes: int32 [4096, 4], P(('sp', 'tp')), may hold values from 0 to 31, all different within a row; in each aligned block of 128 rows (0 to 127, 128 to 255, ...) at most 32 rows name the same one
- route_weight: float32 [4096, 4], P(('sp', 'tp')), may hold values from 0.25 to 1
- expert_gate: bfloat16 [32, 2048, 512], P(('sp', 'tp')), may hold values from -0.125 to 0.125
- expert_up: bfloat16 [32, 2048, 512], P(('sp', 'tp')), may hold values from -0.125 to 0.125
- expert_down: bfloat16 [32, 512, 2048], P(('sp', 'tp')), may hold values from -0.25 to 0.25
- shared_gate: bfloat16 [2048, 512], replicated, may hold values from -0.125 to 0.125
- shared_up: bfloat16 [2048, 512], replicated, may hold values from -0.125 to 0.125
- shared_down: bfloat16 [512, 2048], replicated, may hold values from -0.25 to 0.25
- ffn_gain: bfloat16 [2048], replicated, may hold values from 0.099609375 to 1.8984375
Outputs:
- result: bfloat16 [4096, 2048], P(('sp', 'tp'))
Inputs may be any that keep to these rules, and one draw needn't show every extreme that they name: `gate_cache`: entry (h, j) is the sum of head h's log forget gates over positions 0 to j. `documents`: never falls along the positions; no document has more than 2560 positions. `routes`: each row names 4 different experts; in the rows of one device (aligned blocks of 128 rows) no expert is named more than 32 times, a bound that some block reaches.
All inputs are finite; a program needn't handle non-finite values.
Results may differ from a plain program's by a relative error of at most 0.013.
Values may be sent and summed in bfloat16 or wider, within the bound.
A program may use at most 256 MiB of HBM per device.

v0:
```python
import jax
import jax.numpy as jnp
from jax import lax
from jax.sharding import PartitionSpec as P

HD = 128
residual_scale = 2.0**0.25
norm_epsilon = 1e-05
masked_score = -1e30


def normalize(summed, gain_vector):
    row_mean = jnp.mean(summed, axis=-1, keepdims=True)
    centred = summed - row_mean
    spread = jnp.mean(centred * centred, axis=-1, keepdims=True)
    return (centred * lax.rsqrt(spread + norm_epsilon) * gain_vector.astype(jnp.float32)).astype(
        jnp.bfloat16
    )


def expert_block(arrived, expert_gate, expert_up, expert_down):
    own_count = expert_gate.shape[0]
    grouped = arrived.reshape(-1, own_count, arrived.shape[1], arrived.shape[2])
    gate_part = jnp.einsum(
        "nemd,edf->nemf", grouped, expert_gate, preferred_element_type=jnp.float32
    )
    up_part = jnp.einsum("nemd,edf->nemf", grouped, expert_up, preferred_element_type=jnp.float32)
    hidden = (jax.nn.silu(gate_part) * up_part).astype(jnp.bfloat16)
    produced = jnp.einsum("nemf,efd->nemd", hidden, expert_down, preferred_element_type=jnp.float32)
    return produced.astype(jnp.bfloat16).reshape(arrived.shape)


def local(
    queries,
    keys,
    values,
    gate_cache,
    documents,
    residual,
    out_weight,
    mix_gain,
    routes,
    route_weight,
    expert_gate,
    expert_up,
    expert_down,
    shared_gate,
    shared_up,
    shared_down,
    ffn_gain,
):
    tok_rows = queries.shape[0]
    local_heads = gate_cache.shape[0]
    kv_local = keys.shape[0] // HD
    group_size = local_heads // kv_local
    score_scale = HD ** (-0.5)
    seq_start = lax.axis_index("sp") * tok_rows
    query_pos = seq_start + jnp.arange(tok_rows, dtype=jnp.int32)
    query_last = seq_start + tok_rows - 1
    query_cum = jnp.transpose(gate_cache).reshape(tok_rows, kv_local, group_size)
    grouped_q = queries.reshape(tok_rows, kv_local, group_size, HD)
    all_cache, all_docs = (
        lax.all_gather(gate_cache, "sp", axis=1, tiled=True),
        lax.all_gather(documents.reshape(1, tok_rows), "sp", axis=1, tiled=True),
    )
    doc_line = all_docs[0]
    initial = (
        jnp.full((tok_rows, kv_local, group_size), masked_score, jnp.float32),
        jnp.zeros((tok_rows, kv_local, group_size), jnp.float32),
        jnp.zeros((tok_rows, kv_local, group_size, HD), jnp.float32),
    )
    key_piece = lax.all_gather(keys, "sp", axis=1, tiled=True)
    value_piece = lax.all_gather(values, "sp", axis=1, tiled=True)
    width_keys = key_piece.shape[1]
    key_cum = all_cache.reshape(kv_local, group_size, width_keys)

    def update(state):
        running_max, running_sum, numerator = state
        key_block = key_piece.reshape(kv_local, HD, width_keys)
        value_block = value_piece.reshape(kv_local, HD, width_keys)
        scores = (
            jnp.einsum("qagd,adk->qagk", grouped_q, key_block, preferred_element_type=jnp.float32)
            * score_scale
        )
        scores = scores + query_cum[..., None] - key_cum[None]
        key_pos = jnp.arange(width_keys, dtype=jnp.int32)
        allowed = (key_pos[None, :] <= query_pos[:, None]) & (
            doc_line[None, :] == documents[:, None]
        )
        allowed = allowed[:, None, None, :]
        scores = jnp.where(allowed, scores, masked_score)
        new_max = jnp.maximum(running_max, jnp.max(scores, axis=-1))
        weights = jnp.where(allowed, jnp.exp(scores - new_max[..., None]), 0.0)
        new_sum = jnp.sum(weights, axis=-1)
        added = jnp.einsum(
            "qagk,adk->qagd",
            weights.astype(jnp.bfloat16),
            value_block,
            preferred_element_type=jnp.float32,
        )
        return (new_max, new_sum, added)

    active = (jnp.int32(0) <= query_last) & (doc_line[width_keys - 1] >= documents[0])
    running_max, running_sum, numerator = lax.cond(active, update, lambda state: state, initial)
    attended = (
        (numerator / running_sum[..., None])
        .astype(jnp.bfloat16)
        .reshape(tok_rows, local_heads * HD)
    )
    token_heads = lax.all_to_all(attended, "tp", split_axis=0, concat_axis=1, tiled=True)
    mixed = jnp.dot(token_heads, out_weight, preferred_element_type=jnp.float32)
    mixed = lax.optimization_barrier(mixed.astype(jnp.bfloat16)).astype(jnp.float32)
    settled = normalize(residual_scale * residual.astype(jnp.float32) + mixed, mix_gain)
    row_count = settled.shape[0]
    width_model = settled.shape[1]
    top_count = routes.shape[1]
    expert_total = lax.axis_size(("sp", "tp")) * expert_gate.shape[0]
    capacity = row_count * lax.axis_size("tp") * top_count // expert_total
    chosen_experts = routes.reshape(-1)
    matches = (
        chosen_experts[:, None] == jnp.arange(expert_total, dtype=jnp.int32)[None, :]
    ).astype(jnp.int32)
    ranks = jnp.sum(jnp.cumsum(matches, axis=0) * matches, axis=1) - 1
    slots = chosen_experts * capacity + ranks
    placing = slots[None, :] == jnp.arange(expert_total * capacity, dtype=jnp.int32)[:, None]
    placing = jnp.any(
        placing.reshape(expert_total * capacity, row_count, top_count), axis=2
    ).astype(jnp.bfloat16)
    outgoing = jnp.dot(placing, settled, preferred_element_type=jnp.float32).astype(jnp.bfloat16)
    outgoing = outgoing.reshape(expert_total, capacity, width_model)
    finished = expert_block(
        lax.all_to_all(outgoing, ("sp", "tp"), split_axis=0, concat_axis=0, tiled=True),
        expert_gate,
        expert_up,
        expert_down,
    )
    returned = lax.all_to_all(finished, ("sp", "tp"), split_axis=0, concat_axis=0, tiled=True)
    returned = returned.reshape(expert_total * capacity, width_model)
    picked_rows = jnp.take(returned, slots, axis=0).reshape(row_count, top_count, width_model)
    routed = jnp.einsum("rkd,rk->rd", picked_rows.astype(jnp.float32), route_weight)
    shared_gate_part = jnp.dot(settled, shared_gate, preferred_element_type=jnp.float32)
    shared_up_part = jnp.dot(settled, shared_up, preferred_element_type=jnp.float32)
    shared_hidden = (jax.nn.silu(shared_gate_part) * shared_up_part).astype(jnp.bfloat16)
    shared = jnp.dot(shared_hidden, shared_down, preferred_element_type=jnp.float32)
    return normalize(residual_scale * settled.astype(jnp.float32) + routed + shared, ffn_gain)


def solution(mesh):
    placed = (
        P("sp", "tp"),
        P("tp", "sp"),
        P("tp", "sp"),
        P("tp", "sp"),
        P("sp"),
        P(("sp", "tp"), None),
        P(),
        P(),
        P(("sp", "tp"), None),
        P(("sp", "tp"), None),
        P(("sp", "tp"), None, None),
        P(("sp", "tp"), None, None),
        P(("sp", "tp"), None, None),
        P(),
        P(),
        P(),
        P(),
    )
    return jax.shard_map(
        local, mesh=mesh, in_specs=placed, out_specs=P(("sp", "tp"), None), check_vma=False
    )
```

profile of v0, /device:TPU:0, one launch (start us, length us, event | category | flops | bytes accessed | tf_op | source)
XLA Modules:
  0.0 393.6 jit_solution(2535516395564024456)
XLA Ops:
  6.5 1.7 copy.56
  8.3 0.7 all-gather.7.cloned.1.call-update
  9.0 0.8 copy.59
  10.1 1.2 slice.14
  11.3 42.7 %all-gather.1 = s32[16,1,256]{2,1,0:T(1,128)S(1)} all-gather(s32[1,1,256]{2,1,0:T(1,128)} %bitcast.172), channel_id=2, replica_groups=mesh['sp'=16,'tp'=2] {'sp'}, dimensions={0}, use_global_device_ids=true | all-gather | bytes 17408 | tf_op jit(solution)/shard_map/all_gather | solution.py:64
  54.0 0.6 slice.19
  55.8 0.7 convert_element_type.60
  56.5 1.2 reduce-window.6
  58.3 36.1 %all_gather.14 = f32[4,4096]{1,0:T(4,128)S(1)} all-gather(f32[4,256]{1,0:T(4,128)} %param.22), channel_id=1, replica_groups=mesh['sp'=16,'tp'=2] {'sp'}, dimensions={1}, use_global_device_ids=true | all-gather | bytes 69632 | tf_op jit(solution)/shard_map/all_gather | solution.py:63
  94.4 0.7 compare_and_fusion
  95.1 0.4 fusion.31
  95.4 29.3 %all-gather.7.cloned.1.call-done = bf16[128,4096]{1,0:T(8,128)(2,1)} async-done(((bf16[128,256]{1,0:T(8,128)(2,1)}), bf16[128,4096]{1,0:T(8,128)(2,1)}) %all-gather.7.cloned.1.call-update) | async-done | bytes 1048592 | tf_op jit(solution)/shard_map/all_gather | solution.py:73
  124.7 20.7 %conditional.1 = (f32[256,1,4]{0,2,1:T(4,128)S(1)}, f32[256,1,4,128]{3,0,2,1:T(8,128)S(1)}) conditional(s32[]{:T(128)} %convert_element_type.56, () %tuple.13, (s32[]{:T(128)}, s32[256]{0:T(256)S(1)}, s32[1,4096]{1,0:T(1,128)S(1)}, s32[256]{0:T(256)}, bf16[256,512]{1,0:T(8,128)(2,1)}, /*index=5*/bf16[128,4096]{0,1:T(8,128)(2,1)}, f32[256,4]{0,1:T(4,128)}, ...), branch_computations={%region_0.0_spmd, %region_1.4_spmd} | conditional | flops 2230320384 | bytes 61874252 | solution.py:104
  124.7 2.5 fusion.8
  127.3 5.5 %fusion.3 = (f32[256,4]{0,1:T(4,128)S(1)}, f32[4096,256,4]{1,0,2:T(8,128)S(1)}) fusion(f32[4,4096]{1,0:T(4,128)S(1)} %get-tuple-element.33, f32[256,4]{0,1:T(4,128)} %get-tuple-element.32, pred[256,4096]{0,1:T(8,128)(4,1)S(1)} %fusion.8, bf16[128,4096]{0,1:T(8,128)(2,1)} %get-tuple-element.30, bf16[256,512]{1,0:T(8,128)(2,1)} %get-tuple-element.40), kind=kOutput, calls=%fused_computation.7 | convolution fusion | flops 1094712320 | bytes 19210240 | tf_op jit(solution)/shard_map/cond/branch_1_fun/qagd,adk->qagk/dot_general | solution.py:82
  132.8 6.8 %fusion.9 = f32[256,1,4,128]{3,0,2,1:T(8,128)S(1)} fusion(f32[4096,256,4]{1,0,2:T(8,128)S(1)} %get-tuple-element.44, f32[256,4]{0,1:T(4,128)S(1)} %broadcast_maximum_fusion, f32[4,4096]{1,0:T(4,128)S(1)} %get-tuple-element.33, f32[256,4]{0,1:T(4,128)S(1)} %copy-done.5, pred[256,4096]{0,1:T(8,128)(4,1)S(1)} %fusion.8, bf16[128,4096]{1,0:T(8,128)(2,1)S(1)} %copy-done.9), kind=kOutput, calls=%fused_computation.13 | convolution fusion | flops 1103101952 | bytes 19472384 | tf_op jit(solution)/shard_map/cond/branch_1_fun/qagk,adk->qagd/dot_general | solution.py:95
  139.7 5.8 %fusion.2 = f32[256,4]{0,1:T(4,128)S(1)} fusion(f32[4096,256,4]{1,0,2:T(8,128)S(1)} %get-tuple-element.44, f32[256,4]{0,1:T(4,128)S(1)} %broadcast_maximum_fusion, f32[4,4096]{1,0:T(4,128)S(1)} %get-tuple-element.33, f32[256,4]{0,1:T(4,128)S(1)} %copy-done.5, pred[256,4096]{0,1:T(8,128)(4,1)S(1)} %fusion.8), kind=kLoop, calls=%fused_computation.6 | loop fusion | flops 29359104 | bytes 17903616 | tf_op jit(solution)/shard_map/cond/branch_1_fun/reduce_sum | solution.py:94
  146.0 3.9 %all_to_all.29 = bf16[2,128,512]{2,1,0:T(8,128)(2,1)S(1)} all-to-all(bf16[2,128,512]{2,1,0:T(8,128)(2,1)S(1)} %all_to_all.20), channel_id=1, replica_groups=mesh['sp'=16,'tp'=2] {'tp'}, dimensions={0} | all-to-all | bytes 524288 | tf_op jit(solution)/shard_map/all_to_all | solution.py:110
  150.1 2.9 convolution_convert_fusion.2
  154.0 1.2 convolution_convert_fusion.1
  155.2 96.7 %all_to_all.30 = bf16[32,32,2048]{2,1,0:T(8,128)(2,1)S(1)} all-to-all(bf16[32,32,2048]{2,1,0:T(8,128)(2,1)S(1)} %bitcast.161), channel_id=1, replica_groups=mesh['sp'=16,'tp'=2] {'sp','tp'}, dimensions={0} | all-to-all | bytes 8388608 | tf_op jit(solution)/shard_map/all_to_all | solution.py:132
  252.0 2.0 copy-done.3
  253.9 3.7 fusion.22
  257.7 10.1 %convolution_convert_fusion = bf16[32,32,2048]{2,1,0:T(8,128)(2,1)} fusion(bf16[1,512,2048]{2,1,0:T(8,128)(2,1)S(1)} %copy-done, f32[32,32,512]{2,1,0:T(8,128)} %fusion.22, bf16[32,32,2048]{2,1,0:T(8,128)(2,1)} %copy-done.3, bf16[1,2048,512]{2,1,0:T(8,128)(2,1)} %param.29), kind=kOutput, calls=%fused_computation.24 | convolution fusion | flops 4300210176 | bytes 14680064 | tf_op jit(solution)/shard_map/nemf,efd->nemd/dot_general | solution.py:29
  267.7 4.0 %all-to-all-start.2 = ((bf16[32,32,2048]{2,1,0:T(8,128)(2,1)}), bf16[32,32,2048]{2,1,0:T(8,128)(2,1)}, u32[]{:S(2)}, u32[]{:S(2)}) async-start(bf16[32,32,2048]{2,1,0:T(8,128)(2,1)} %convolution_convert_fusion), calls=%async_computation.2 | async-start | bytes 8388608 | tf_op jit(solution)/shard_map/all_to_all | solution.py:137
  272.4 2.0 fusion.58
  274.4 91.0 %all-to-all-done.2 = bf16[32,32,2048]{2,1,0:T(8,128)(2,1)} async-done(((bf16[32,32,2048]{2,1,0:T(8,128)(2,1)}), bf16[32,32,2048]{2,1,0:T(8,128)(2,1)}, u32[]{:S(2)}, u32[]{:S(2)}) %all-to-all-start.2) | async-done | bytes 4194336 | tf_op jit(solution)/shard_map/all_to_all | solution.py:137
  365.5 8.0 %gather_fusion = bf16[512,2048]{1,0:T(8,128)(2,1)} fusion(bf16[1024,2048]{1,0:T(8,128)(2,1)} %bitcast.35, s32[1024]{0:T(1024)S(1)} %pad_clamp_fusion), kind=kCustom, calls=%fused_computation | custom fusion | bytes 4196352 | tf_op jit(solution)/shard_map/jit(_take)/gather | solution.py:139
  373.5 4.1 %gather.7 = bf16[128,4,2048]{2,1,0:T(4,128)(2,1)} reshape(bf16[512,2048]{1,0:T(8,128)(2,1)} %gather_fusion) | data formatting | bytes 4194304 | tf_op jit(solution)/shard_map/jit(_take)/gather | solution.py:139
  377.6 3.9 fusion.29
  381.5 4.0 %fusion.57 = (f32[128]{0:T(128)S(1)}, f32[128,2048]{1,0:T(8,128)S(1)}) fusion(bf16[512,2048]{1,0:T(8,128)(2,1)} %param.34, bf16[128,2048]{1,0:T(8,128)(2,1)} %copy-done.1, bf16[2048,512]{1,0:T(8,128)(2,1)} %param.33, f32[128,512]{1,0:T(8,128)S(1)} %fusion.58, f32[128,1,2048]{2,1,0:T(1,128)} %fusion.29), kind=kOutput, calls=%fused_computation.85 | convolution fusion | flops 538574720 | bytes 7078400 | tf_op jit(solution)/shard_map/dot_general | solution.py:144
  385.7 1.0 multiply_convert_fusion
  (56 shorter events, 3.3 us)
Async XLA Ops:
  6.5 251.1 %copy-start = (bf16[1,512,2048]{2,1,0:T(8,128)(2,1)S(1)}, bf16[1,512,2048]{2,1,0:T(8,128)(2,1)}, u32[]{:S(2)}) copy-start(bf16[1,512,2048]{2,1,0:T(8,128)(2,1)} %param.31) | copy-start | bytes 6291460
  6.5 88.9 %all-gather.5.cloned.1.call-start = ((), (), s32[]{:S(2)}) async-start(), calls=%async_computation.3 | async-start | bytes 1114112 | tf_op jit(solution)/shard_map/all_gather | solution.py:72
  8.3 116.4 %all-gather.7.cloned.1.call-start = ((), (), s32[]{:S(2)}) async-start(), calls=%async_computation.4 | async-start | bytes 1114112 | tf_op jit(solution)/shard_map/all_gather | solution.py:73
  127.3 5.5 %copy-start.5 = (f32[256,4]{0,1:T(4,128)S(1)}, f32[256,4]{0,1:T(4,128)}, u32[]{:S(2)}) copy-start(f32[256,4]{0,1:T(4,128)} %get-tuple-element.32) | copy-start | bytes 12292 | tf_op jit(solution)/shard_map/cond
  127.3 5.5 %copy-start.9 = (bf16[128,4096]{1,0:T(8,128)(2,1)S(1)}, bf16[128,4096]{1,0:T(8,128)(2,1)}, u32[]{:S(2)}) copy-start(bf16[128,4096]{1,0:T(8,128)(2,1)} %get-tuple-element.34) | copy-start | bytes 3145732 | tf_op jit(solution)/shard_map/cond
  145.5 7.6 %copy-start.2 = (bf16[128,2048]{1,0:T(8,128)(2,1)S(1)}, bf16[128,2048]{1,0:T(8,128)(2,1)}, u32[]{:S(2)}) copy-start(bf16[128,2048]{1,0:T(8,128)(2,1)} %param.24) | copy-start | bytes 1572868
  154.0 118.4 %copy-start.1 = (bf16[128,2048]{1,0:T(8,128)(2,1)}, bf16[128,2048]{1,0:T(8,128)(2,1)S(1)}, u32[]{:S(2)}) copy-start(bf16[128,2048]{1,0:T(8,128)(2,1)S(1)} %multiply_convert_fusion.1) | copy-start | bytes 1572868
  155.2 98.7 %copy-start.8 = (bf16[1,2048,512]{2,1,0:T(8,128)(2,1)S(1)}, bf16[1,2048,512]{2,1,0:T(8,128)(2,1)}, u32[]{:S(2)}) copy-start(bf16[1,2048,512]{2,1,0:T(8,128)(2,1)} %param.30) | copy-start | bytes 6291460
  252.0 2.0 copy-start.3
  267.7 4.0 %copy-start.4 = (s32[128,4]{0,1:T(4,128)S(1)}, s32[128,4]{0,1:T(4,128)}, u32[]{:S(2)}) copy-start(s32[128,4]{0,1:T(4,128)} %param.27) | copy-start | bytes 6148
  267.7 4.4 %copy-start.7 = (f32[128,4]{0,1:T(4,128)S(1)}, f32[128,4]{0,1:T(4,128)}, u32[]{:S(2)}) copy-start(f32[128,4]{0,1:T(4,128)} %param.28) | copy-start | bytes 6148
  267.7 4.6 %copy-start.6 = (bf16[2048]{0:T(1024)(128)(2,1)S(1)}, bf16[2048]{0:T(1024)(128)(2,1)}, u32[]{:S(2)}) copy-start(bf16[2048]{0:T(1024)(128)(2,1)} %param.35) | copy-start | bytes 12292
  267.7 97.7 %all-to-all-start.2 = ((bf16[32,32,2048]{2,1,0:T(8,128)(2,1)}), bf16[32,32,2048]{2,1,0:T(8,128)(2,1)}, u32[]{:S(2)}, u32[]{:S(2)}) async-start(bf16[32,32,2048]{2,1,0:T(8,128)(2,1)} %convolution_convert_fusion), calls=%async_computation.2 | async-start | bytes 8388608 | tf_op jit(solution)/shard_map/all_to_all | solution.py:137
Sparse Core Ops, SparseCore 0:
  10.1 57.9 all-gather.4
  70.8 53.9 all-gather.6
where the time goes:
time: 394 us
  blocking collectives  180 us (46%)
  waiting for transfers between devices  121 us (31%)
  matrix products  40.2 us (10%)
  local copies, waits for them, and re-layouts  20.1 us (5%)
  between operations  14.9 us (4%)
  other arithmetic  13.8 us (4%)
  starting transfers between devices  4.06 us (1%)
    all_to_all x1, blocking collectives, local(): lax.all_to_all(outgoing, ('sp', 'tp'), split_axis=0, concat_axis=0, tiled...  96.7 us
    all_to_all x1, waiting for transfers between devices, local(): lax.all_to_all(finished, ('sp', 'tp'), split_axis=0, concat_axis=0, tiled...  91 us
    all_gather x1, blocking collectives, local(): lax.all_gather(documents.reshape(1, tok_rows), 'sp', axis=1, tiled=True)  42.7 us
    all_gather x1, blocking collectives, local(): lax.all_gather(gate_cache, 'sp', axis=1, tiled=True)  36.1 us
    all_gather x1, waiting for transfers between devices, local(): value_piece = lax.all_gather(values, 'sp', axis=1, tiled=True)  29.3 us
    gather x2, local copies, waits for them, and re-layouts, local(): jnp.take(returned, slots, axis=0).reshape(row_count, top_count, width_model)  12.1 us
    dot_general x1, matrix products, expert_block(): jnp.einsum('nemf,efd->nemd', hidden, expert_down, preferred_element_type=...  10.1 us
  transfers between devices with their start and end apart: 3, of which 2 were waited for; matrix products, arithmetic and copies ran while one was open for 2% of the time, Pallas kernels for 0%

commit v1 on v0

--- a/solution.py
+++ b/solution.py
@@ -60,7 +60,7 @@
     query_cum = jnp.transpose(gate_cache).reshape(tok_rows, kv_local, group_size)
     grouped_q = queries.reshape(tok_rows, kv_local, group_size, HD)
     all_cache, all_docs = (
-        lax.all_gather(gate_cache, "sp", axis=1, tiled=True),
+        jnp.concatenate(lax.all_gather(gate_cache, "sp"), axis=1),
         lax.all_gather(documents.reshape(1, tok_rows), "sp", axis=1, tiled=True),
     )
     doc_line = all_docs[0]

time: 394 us -> 394 us (level)
  no operation moved by 1% of the time
where the time goes in v1:
time: 394 us
  blocking collectives  180 us (46%)
  waiting for transfers between devices  121 us (31%)
  matrix products  40.2 us (10%)
  local copies, waits for them, and re-layouts  20.1 us (5%)
  between operations  14.9 us (4%)
  other arithmetic  13.8 us (4%)
  starting transfers between devices  4.06 us (1%)
    all_to_all x1, blocking collectives, local(): lax.all_to_all(outgoing, ('sp', 'tp'), split_axis=0, concat_axis=0, tiled...  96.7 us
    all_to_all x1, waiting for transfers between devices, local(): lax.all_to_all(finished, ('sp', 'tp'), split_axis=0, concat_axis=0, tiled...  91 us
    all_gather x1, blocking collectives, local(): lax.all_gather(documents.reshape(1, tok_rows), 'sp', axis=1, tiled=True)  42.7 us
    all_gather x1, blocking collectives, local(): lax.all_gather(gate_cache, 'sp')  36.1 us
    all_gather x1, waiting for transfers between devices, local(): value_piece = lax.all_gather(values, 'sp', axis=1, tiled=True)  29.3 us
    gather x2, local copies, waits for them, and re-layouts, local(): jnp.take(returned, slots, axis=0).reshape(row_count, top_count, width_model)  12.1 us
    dot_general x1, matrix products, expert_block(): jnp.einsum('nemf,efd->nemd', hidden, expert_down, preferred_element_type=...  10.1 us
  transfers between devices with their start and end apart: 3, of which 2 were waited for; matrix products, arithmetic and copies ran while one was open for 2% of the time, Pallas kernels for 0%

profile of v1, /device:TPU:0, one launch (start us, length us, event | category | flops | bytes accessed | tf_op | source)
XLA Modules:
  0.0 393.6 jit_solution(11205409485144801095)
XLA Ops:
  6.5 1.7 copy.58
  8.3 0.7 all-gather.9.cloned.1.call-update
  9.0 0.8 copy.62
  10.1 1.2 slice.14
  11.3 42.7 %all-gather.2 = s32[16,1,256]{2,1,0:T(1,128)S(1)} all-gather(s32[1,1,256]{2,1,0:T(1,128)} %bitcast.180), channel_id=2, replica_groups=mesh['sp'=16,'tp'=2] {'sp'}, dimensions={0}, use_global_device_ids=true | all-gather | bytes 17408 | tf_op jit(solution)/shard_map/all_gather | solution.py:64
  54.0 0.6 slice.19
  55.8 0.7 convert_element_type.60
  56.5 1.2 reduce-window.6
  58.3 36.1 %all-gather.3 = f32[16,4,256]{2,1,0:T(4,128)S(1)} all-gather(f32[1,4,256]{2,1,0:T(4,128)} %bitcast.175), channel_id=3, replica_groups=mesh['sp'=16,'tp'=2] {'sp'}, dimensions={0}, use_global_device_ids=true | all-gather | bytes 69632 | tf_op jit(solution)/shard_map/all_gather | solution.py:63
  94.4 0.7 compare_and_fusion
  95.1 0.4 fusion.31
  95.4 29.3 %all-gather.9.cloned.1.call-done = bf16[128,4096]{1,0:T(8,128)(2,1)} async-done(((bf16[128,256]{1,0:T(8,128)(2,1)}), bf16[128,4096]{1,0:T(8,128)(2,1)}) %all-gather.9.cloned.1.call-update) | async-done | bytes 1048592 | tf_op jit(solution)/shard_map/all_gather | solution.py:73
  124.7 20.7 %conditional.1 = (f32[256,1,4]{0,2,1:T(4,128)S(1)}, f32[256,1,4,128]{3,0,2,1:T(8,128)S(1)}) conditional(s32[]{:T(128)} %convert_element_type.56, () %tuple.13, (s32[]{:T(128)}, s32[256]{0:T(256)S(1)}, s32[1,4096]{1,0:T(1,128)S(1)}, s32[256]{0:T(256)}, bf16[256,512]{1,0:T(8,128)(2,1)}, /*index=5*/bf16[128,4096]{0,1:T(8,128)(2,1)}, f32[256,4]{0,1:T(4,128)}, ...), branch_computations={%region_0.0_spmd, %region_1.4_spmd} | conditional | flops 2230320384 | bytes 61874252 | solution.py:104
  124.7 2.5 fusion.8
  127.3 5.5 %fusion.3 = (f32[256,4]{0,1:T(4,128)S(1)}, f32[4096,256,4]{1,0,2:T(8,128)S(1)}) fusion(f32[4,4096]{1,0:T(4,128)S(1)} %bitcast.168, f32[256,4]{0,1:T(4,128)} %get-tuple-element.32, pred[256,4096]{0,1:T(8,128)(4,1)S(1)} %fusion.8, bf16[128,4096]{0,1:T(8,128)(2,1)} %get-tuple-element.30, bf16[256,512]{1,0:T(8,128)(2,1)} %get-tuple-element.40), kind=kOutput, calls=%fused_computation.7 | convolution fusion | flops 1094712320 | bytes 19210240 | tf_op jit(solution)/shard_map/cond/branch_1_fun/qagd,adk->qagk/dot_general | solution.py:82
  132.8 6.8 %fusion.9 = f32[256,1,4,128]{3,0,2,1:T(8,128)S(1)} fusion(f32[4096,256,4]{1,0,2:T(8,128)S(1)} %get-tuple-element.71, f32[256,4]{0,1:T(4,128)S(1)} %broadcast_maximum_fusion, f32[4,4096]{1,0:T(4,128)S(1)} %bitcast.169, f32[256,4]{0,1:T(4,128)S(1)} %copy-done.5, pred[256,4096]{0,1:T(8,128)(4,1)S(1)} %fusion.8, bf16[128,4096]{1,0:T(8,128)(2,1)S(1)} %copy-done.9), kind=kOutput, calls=%fused_computation.13 | convolution fusion | flops 1103101952 | bytes 19472384 | tf_op jit(solution)/shard_map/cond/branch_1_fun/qagk,adk->qagd/dot_general | solution.py:95
  139.7 5.8 %fusion.2 = f32[256,4]{0,1:T(4,128)S(1)} fusion(f32[4096,256,4]{1,0,2:T(8,128)S(1)} %get-tuple-element.71, f32[256,4]{0,1:T(4,128)S(1)} %broadcast_maximum_fusion, f32[4,4096]{1,0:T(4,128)S(1)} %bitcast.170, f32[256,4]{0,1:T(4,128)S(1)} %copy-done.5, pred[256,4096]{0,1:T(8,128)(4,1)S(1)} %fusion.8), kind=kLoop, calls=%fused_computation.6 | loop fusion | flops 29359104 | bytes 17903616 | tf_op jit(solution)/shard_map/cond/branch_1_fun/reduce_sum | solution.py:94
  146.0 3.9 %all_to_all.29 = bf16[2,128,512]{2,1,0:T(8,128)(2,1)S(1)} all-to-all(bf16[2,128,512]{2,1,0:T(8,128)(2,1)S(1)} %all_to_all.20), channel_id=1, replica_groups=mesh['sp'=16,'tp'=2] {'tp'}, dimensions={0} | all-to-all | bytes 524288 | tf_op jit(solution)/shard_map/all_to_all | solution.py:110
  150.1 2.9 convolution_convert_fusion.2
  154.0 1.2 convolution_convert_fusion.1
  155.2 96.7 %all_to_all.30 = bf16[32,32,2048]{2,1,0:T(8,128)(2,1)S(1)} all-to-all(bf16[32,32,2048]{2,1,0:T(8,128)(2,1)S(1)} %bitcast.164), channel_id=1, replica_groups=mesh['sp'=16,'tp'=2] {'sp','tp'}, dimensions={0} | all-to-all | bytes 8388608 | tf_op jit(solution)/shard_map/all_to_all | solution.py:132
  252.0 2.0 copy-done.3
  253.9 3.7 fusion.22
  257.7 10.1 %convolution_convert_fusion = bf16[32,32,2048]{2,1,0:T(8,128)(2,1)} fusion(bf16[1,512,2048]{2,1,0:T(8,128)(2,1)S(1)} %copy-done, f32[32,32,512]{2,1,0:T(8,128)} %fusion.22, bf16[32,32,2048]{2,1,0:T(8,128)(2,1)} %copy-done.3, bf16[1,2048,512]{2,1,0:T(8,128)(2,1)} %param.29), kind=kOutput, calls=%fused_computation.24 | convolution fusion | flops 4300210176 | bytes 14680064 | tf_op jit(solution)/shard_map/nemf,efd->nemd/dot_general | solution.py:29
  267.7 4.0 %all-to-all-start.2 = ((bf16[32,32,2048]{2,1,0:T(8,128)(2,1)}), bf16[32,32,2048]{2,1,0:T(8,128)(2,1)}, u32[]{:S(2)}, u32[]{:S(2)}) async-start(bf16[32,32,2048]{2,1,0:T(8,128)(2,1)} %convolution_convert_fusion), calls=%async_computation.2 | async-start | bytes 8388608 | tf_op jit(solution)/shard_map/all_to_all | solution.py:137
  272.4 2.0 fusion.58
  274.4 91.0 %all-to-all-done.2 = bf16[32,32,2048]{2,1,0:T(8,128)(2,1)} async-done(((bf16[32,32,2048]{2,1,0:T(8,128)(2,1)}), bf16[32,32,2048]{2,1,0:T(8,128)(2,1)}, u32[]{:S(2)}, u32[]{:S(2)}) %all-to-all-start.2) | async-done | bytes 4194336 | tf_op jit(solution)/shard_map/all_to_all | solution.py:137
  365.5 8.0 %gather_fusion = bf16[512,2048]{1,0:T(8,128)(2,1)} fusion(bf16[1024,2048]{1,0:T(8,128)(2,1)} %bitcast.38, s32[1024]{0:T(1024)S(1)} %pad_clamp_fusion), kind=kCustom, calls=%fused_computation | custom fusion | bytes 4196352 | tf_op jit(solution)/shard_map/jit(_take)/gather | solution.py:139
  373.5 4.1 %gather.7 = bf16[128,4,2048]{2,1,0:T(4,128)(2,1)} reshape(bf16[512,2048]{1,0:T(8,128)(2,1)} %gather_fusion) | data formatting | bytes 4194304 | tf_op jit(solution)/shard_map/jit(_take)/gather | solution.py:139
  377.6 3.9 fusion.29
  381.5 4.0 %fusion.57 = (f32[128]{0:T(128)S(1)}, f32[128,2048]{1,0:T(8,128)S(1)}) fusion(bf16[512,2048]{1,0:T(8,128)(2,1)} %param.34, bf16[128,2048]{1,0:T(8,128)(2,1)} %copy-done.1, bf16[2048,512]{1,0:T(8,128)(2,1)} %param.33, f32[128,512]{1,0:T(8,128)S(1)} %fusion.58, f32[128,1,2048]{2,1,0:T(1,128)} %fusion.29), kind=kOutput, calls=%fused_computation.85 | convolution fusion | flops 538574720 | bytes 7078400 | tf_op jit(solution)/shard_map/dot_general | solution.py:144
  385.7 1.0 multiply_convert_fusion
  (56 shorter events, 3.3 us)
Async XLA Ops:
  6.5 251.1 %copy-start = (bf16[1,512,2048]{2,1,0:T(8,128)(2,1)S(1)}, bf16[1,512,2048]{2,1,0:T(8,128)(2,1)}, u32[]{:S(2)}) copy-start(bf16[1,512,2048]{2,1,0:T(8,128)(2,1)} %param.31) | copy-start | bytes 6291460
  6.5 88.9 %all-gather.7.cloned.1.call-start = ((), (), s32[]{:S(2)}) async-start(), calls=%async_computation.3 | async-start | bytes 1114112 | tf_op jit(solution)/shard_map/all_gather | solution.py:72
  8.3 116.4 %all-gather.9.cloned.1.call-start = ((), (), s32[]{:S(2)}) async-start(), calls=%async_computation.4 | async-start | bytes 1114112 | tf_op jit(solution)/shard_map/all_gather | solution.py:73
  127.3 5.5 %copy-start.5 = (f32[256,4]{0,1:T(4,128)S(1)}, f32[256,4]{0,1:T(4,128)}, u32[]{:S(2)}) copy-start(f32[256,4]{0,1:T(4,128)} %get-tuple-element.32) | copy-start | bytes 12292 | tf_op jit(solution)/shard_map/cond
  127.3 5.5 %copy-start.9 = (bf16[128,4096]{1,0:T(8,128)(2,1)S(1)}, bf16[128,4096]{1,0:T(8,128)(2,1)}, u32[]{:S(2)}) copy-start(bf16[128,4096]{1,0:T(8,128)(2,1)} %get-tuple-element.34) | copy-start | bytes 3145732 | tf_op jit(solution)/shard_map/cond
  145.5 7.6 %copy-start.2 = (bf16[128,2048]{1,0:T(8,128)(2,1)S(1)}, bf16[128,2048]{1,0:T(8,128)(2,1)}, u32[]{:S(2)}) copy-start(bf16[128,2048]{1,0:T(8,128)(2,1)} %param.24) | copy-start | bytes 1572868
  154.0 118.4 %copy-start.1 = (bf16[128,2048]{1,0:T(8,128)(2,1)}, bf16[128,2048]{1,0:T(8,128)(2,1)S(1)}, u32[]{:S(2)}) copy-start(bf16[128,2048]{1,0:T(8,128)(2,1)S(1)} %multiply_convert_fusion.1) | copy-start | bytes 1572868
  155.2 98.7 %copy-start.8 = (bf16[1,2048,512]{2,1,0:T(8,128)(2,1)S(1)}, bf16[1,2048,512]{2,1,0:T(8,128)(2,1)}, u32[]{:S(2)}) copy-start(bf16[1,2048,512]{2,1,0:T(8,128)(2,1)} %param.30) | copy-start | bytes 6291460
  252.0 2.0 copy-start.3
  267.7 4.0 %copy-start.4 = (s32[128,4]{0,1:T(4,128)S(1)}, s32[128,4]{0,1:T(4,128)}, u32[]{:S(2)}) copy-start(s32[128,4]{0,1:T(4,128)} %param.27) | copy-start | bytes 6148
  267.7 4.4 %copy-start.7 = (f32[128,4]{0,1:T(4,128)S(1)}, f32[128,4]{0,1:T(4,128)}, u32[]{:S(2)}) copy-start(f32[128,4]{0,1:T(4,128)} %param.28) | copy-start | bytes 6148
  267.7 4.6 %copy-start.6 = (bf16[2048]{0:T(1024)(128)(2,1)S(1)}, bf16[2048]{0:T(1024)(128)(2,1)}, u32[]{:S(2)}) copy-start(bf16[2048]{0:T(1024)(128)(2,1)} %param.35) | copy-start | bytes 12292
  267.7 97.7 %all-to-all-start.2 = ((bf16[32,32,2048]{2,1,0:T(8,128)(2,1)}), bf16[32,32,2048]{2,1,0:T(8,128)(2,1)}, u32[]{:S(2)}, u32[]{:S(2)}) async-start(bf16[32,32,2048]{2,1,0:T(8,128)(2,1)} %convolution_convert_fusion), calls=%async_computation.2 | async-start | bytes 8388608 | tf_op jit(solution)/shard_map/all_to_all | solution.py:137
Sparse Core Ops, SparseCore 0:
  10.1 57.9 all-gather.6
  70.8 53.9 all-gather.8
